TPU v7x, 32 devices: a whole 2x2x4 slice. The times are simulated.
32 devices in a mesh: dp: 4 (over y, x), kv: 4 (over z), tp: 2 (over core).
Axes of the slice: x: 2, y: 2, z: 4, core: 2. Of those that a mesh axis runs over, the one named last changes fastest.
Arguments:
- tokens: bfloat16 [128, 2048], P('dp', ('kv', 'tp')), may hold values from -100 to 100
- delta_state: float32 [128, 8, 128, 128], P(('dp', 'kv'), 'tp'), may hold values from -0.6 to 0.6
- gain_in: bfloat16 [2048], P('kv'), may hold values from 0.099609375 to 1.8984375
- w_query: bfloat16 [2048, 1024], P('kv', 'tp'), may hold values from -0.125 to 0.125
- w_key: bfloat16 [2048, 1024], P('kv', 'tp'), may hold values from -0.125 to 0.125
- w_value: bfloat16 [2048, 1024], P('kv', 'tp'), may hold values from -0.125 to 0.125
- w_out_gate: bfloat16 [2048, 1024], P('kv', 'tp'), may hold values from -0.125 to 0.125
- w_beta: bfloat16 [2048, 8], P('kv'), may hold values from -0.125 to 0.125
- w_decay: bfloat16 [2048, 8], P('kv'), may hold values from -0.125 to 0.125
- decay_rate: float32 [8], P('tp'), may hold values from 0.05 to 3
- head_gain: float32 [128], replicated, may hold values from 0.1 to 1.9
- w_mix: bfloat16 [1024, 2048], P('tp', 'kv'), may hold values from -0.1875 to 0.1875
- gain_mid: bfloat16 [2048], P('kv'), may hold values from 0.099609375 to 1.8984375
- w_gate: bfloat16 [2048, 5632], P('tp', 'kv'), may hold values from -0.125 to 0.125
- w_up: bfloat16 [2048, 5632], P('tp', 'kv'), may hold values from -0.125 to 0.125
- w_down: bfloat16 [5632, 2048], P('kv', 'tp'), may hold values from -0.078125 to 0.078125
Outputs:
- layer_out: bfloat16 [128, 2048], P('dp', ('kv', 'tp'))
- next_state: float32 [128, 8, 128, 128], P(('dp', 'kv'), 'tp')
All inputs are finite; a program needn't handle non-finite values.
Results may differ from a plain program's by a relative error of at most 0.0095.
Values may be sent and summed in bfloat16 or wider, within the bound.
A program may use at most 64 MiB of HBM per device.

v0:
```python
import jax
import jax.numpy as jnp
from jax import lax
from jax.sharding import PartitionSpec as P

D = 2048
HEAD_DIM = 128


norm_epsilon = 1e-06


def unit_rows(vector):
    return vector * lax.rsqrt(jnp.sum(vector * vector, axis=-1, keepdims=True) + norm_epsilon)


def mixer_core(
    query_lin, key_lin, value_lin, gate_lin, beta_lin, decay_lin, delta_state, decay_rate, head_gain
):
    seq_count = query_lin.shape[0]
    head_count = beta_lin.shape[1]
    shaped = lambda matrix: matrix.reshape(seq_count, head_count, HEAD_DIM)
    query = unit_rows(jax.nn.silu(shaped(query_lin))) * HEAD_DIM ** (-0.5)
    key_vec = unit_rows(jax.nn.silu(shaped(key_lin)))
    value_vec = jax.nn.silu(shaped(value_lin))
    write_rate = jax.nn.sigmoid(beta_lin)
    keep_rate = jnp.exp(-decay_rate[None, :] * jax.nn.softplus(decay_lin))
    recalled = jnp.einsum("bhkv,bhk->bhv", delta_state, key_vec, precision=lax.Precision.HIGHEST)
    correction = write_rate[..., None] * (value_vec - keep_rate[..., None] * recalled)
    next_state = (
        keep_rate[..., None, None] * delta_state + key_vec[..., :, None] * correction[..., None, :]
    )
    readout = jnp.einsum("bhkv,bhk->bhv", next_state, query, precision=lax.Precision.HIGHEST)
    readout = readout * lax.rsqrt(
        jnp.mean(readout * readout, axis=-1, keepdims=True) + norm_epsilon
    )
    readout = readout * head_gain * jax.nn.silu(shaped(gate_lin))
    return (readout.reshape(seq_count, head_count * HEAD_DIM).astype(jnp.bfloat16), next_state)


def local(
    tokens,
    delta_state,
    gain_in,
    w_query,
    w_key,
    w_value,
    w_out_gate,
    w_beta,
    w_decay,
    decay_rate,
    head_gain,
    w_mix,
    gain_mid,
    w_gate,
    w_up,
    w_down,
):
    group_size = lax.axis_size("kv")
    group_pos = lax.axis_index("kv")
    core_pos = lax.axis_index("tp")
    all_rows = tokens.shape[0]
    own_rows = all_rows // group_size
    own_first = group_pos * own_rows
    feature_count = tokens.shape[1]
    head_count = w_query.shape[1] // HEAD_DIM
    width_dev = w_query.shape[1]
    token_float = tokens.astype(jnp.float32)
    sum_squares = jnp.sum(token_float * token_float, axis=1, keepdims=True)
    whole_rows, square_pair = (
        lax.all_gather(tokens, "tp", axis=1, tiled=True),
        lax.all_gather(sum_squares.astype(jnp.bfloat16), "tp", axis=1, tiled=True).astype(
            sum_squares.dtype
        ),
    )
    square_total = lax.psum(jnp.sum(square_pair, axis=1), "kv")
    row_scale = lax.rsqrt(square_total / D + norm_epsilon)
    normed = (whole_rows.astype(jnp.float32) * gain_in.astype(jnp.float32)).astype(jnp.bfloat16)
    beta_cols = lax.dynamic_slice_in_dim(w_beta, core_pos * head_count, head_count, 1)
    decay_cols = lax.dynamic_slice_in_dim(w_decay, core_pos * head_count, head_count, 1)
    row_block = normed
    results = [
        jnp.dot(row_block, weight, preferred_element_type=jnp.float32)
        for weight in (w_query, w_key, w_value, w_out_gate, beta_cols, decay_cols)
    ]
    summand = jnp.concatenate(results, axis=1)
    projected = lax.psum_scatter(
        summand.astype(jnp.bfloat16), "kv", scatter_dimension=0, tiled=True
    ).astype(jnp.float32)
    projected = projected * lax.dynamic_slice_in_dim(row_scale, own_first, own_rows, 0)[:, None]
    mixed, next_state = mixer_core(
        projected[:, :width_dev],
        projected[:, width_dev : 2 * width_dev],
        projected[:, 2 * width_dev : 3 * width_dev],
        projected[:, 3 * width_dev : 4 * width_dev],
        projected[:, 4 * width_dev : 4 * width_dev + head_count],
        projected[:, 4 * width_dev + head_count :],
        delta_state,
        decay_rate,
        head_gain,
    )
    attn_part = jnp.dot(
        lax.all_gather(mixed, "kv", axis=0, tiled=True), w_mix, preferred_element_type=jnp.float32
    )
    attn = lax.psum_scatter(
        attn_part.astype(jnp.bfloat16), "tp", scatter_dimension=1, tiled=True
    ).astype(jnp.float32)
    middle_own = (token_float + attn).astype(jnp.bfloat16)
    middle_float = middle_own.astype(jnp.float32)
    mid_squares = jnp.sum(middle_float * middle_float, axis=1, keepdims=True)
    gain_own = lax.dynamic_slice_in_dim(gain_mid, core_pos * feature_count, feature_count, 0)
    normed_own = (middle_float * gain_own.astype(jnp.float32)).astype(jnp.bfloat16)
    normed_half, square_parts = (
        lax.all_gather(normed_own, "kv", axis=1, tiled=True),
        lax.all_gather(mid_squares.astype(jnp.bfloat16), "kv", axis=1, tiled=True).astype(
            mid_squares.dtype
        ),
    )
    mid_total = lax.psum(jnp.sum(square_parts, axis=1), "tp")
    mid_scale = lax.rsqrt(mid_total / D + norm_epsilon)
    hidden_dev = w_gate.shape[1]
    row_block = normed_half
    summand = jnp.concatenate(
        [
            jnp.dot(row_block, w_gate, preferred_element_type=jnp.float32),
            jnp.dot(row_block, w_up, preferred_element_type=jnp.float32),
        ],
        axis=1,
    )
    gate_up = lax.psum(summand.astype(jnp.bfloat16), "tp").astype(jnp.float32)
    gate_up = gate_up * mid_scale[:, None]
    activated = (jax.nn.silu(gate_up[:, :hidden_dev]) * gate_up[:, hidden_dev:]).astype(
        jnp.bfloat16
    )
    down_local = jnp.dot(activated, w_down, preferred_element_type=jnp.float32)
    down_part = lax.psum_scatter(
        down_local.astype(jnp.bfloat16), "kv", scatter_dimension=1, tiled=True
    ).astype(jnp.float32)
    layer_out = (middle_float + down_part).astype(jnp.bfloat16)
    return (layer_out, next_state)


def solution(mesh):
    in_specs = (
        P("dp", ("kv", "tp")),
        P(("dp", "kv"), "tp", None, None),
        P("kv"),
        P("kv", "tp"),
        P("kv", "tp"),
        P("kv", "tp"),
        P("kv", "tp"),
        P("kv", None),
        P("kv", None),
        P("tp"),
        P(),
        P("tp", "kv"),
        P("kv"),
        P("tp", "kv"),
        P("tp", "kv"),
        P("kv", "tp"),
    )
    out_specs = (P("dp", ("kv", "tp")), P(("dp", "kv"), "tp", None, None))
    return jax.shard_map(local, mesh=mesh, in_specs=in_specs, out_specs=out_specs, check_vma=False)
```

profile of v0, /device:TPU:0, one launch (start us, length us, event | category | flops | bytes accessed | tf_op | source)
XLA Modules:
  0.0 164.7 jit_solution(10898741676465725415)
XLA Ops:
  7.2 0.0 copy-start
  7.2 0.0 copy-start.10
  7.2 0.0 copy-start.5
  7.2 0.0 all-reduce.6.cloned.1.call-start
  7.3 0.8 convert_element_type.92
  8.1 2.3 %all_gather.15 = bf16[32,512]{1,0:T(8,128)(2,1)S(1)} all-gather(bf16[32,256]{1,0:T(8,128)(2,1)} %param.16), channel_id=1, replica_groups=mesh['dp'=4,'kv'=4,'tp'=2] {'tp'}, dimensions={1}, use_global_device_ids=true | all-gather | bytes 49152 | tf_op jit(solution)/shard_map/all_gather | solution.py:71
  10.4 0.8 convolution_convert_fusion.9
  11.2 0.8 convolution_convert_fusion.8
  12.0 0.1 copy.31
  12.2 0.1 copy.30
  12.3 1.2 convolution_convert_fusion.6
  13.5 1.2 convolution_convert_fusion.5
  14.7 1.2 convolution_convert_fusion.4
  16.0 1.2 convolution_convert_fusion.7
  17.2 0.8 concatenate.8
  18.0 0.0 all-reduce.6.cloned.1.call-update
  18.0 0.0 reduce-scatter.3.cloned.1.call-start
  18.1 0.1 fusion.3
  18.2 1.8 %all-gather = bf16[2,1,32]{2,1,0:T(2,128)(2,1)S(1)} all-gather(bf16[1,1,32]{2,1,0:T(2,128)(2,1)S(1)} %bitcast.72), channel_id=1, replica_groups=mesh['dp'=4,'kv'=4,'tp'=2] {'tp'}, dimensions={0}, use_global_device_ids=true | all-gather | bytes 192 | tf_op jit(solution)/shard_map/all_gather | solution.py:72
  20.0 13.3 %psum.21 = f32[32]{0:T(128)S(1)} all-reduce(f32[32]{0:T(128)S(1)} %convert_reduce_fusion.1), channel_id=1, replica_groups=mesh['dp'=4,'kv'=4,'tp'=2] {'kv'}, use_global_device_ids=true, to_apply=%region_3.0 | all-reduce | flops 32 | bytes 256 | tf_op jit(solution)/shard_map/psum | solution.py:76
  33.3 0.6 dynamic-slice
  34.6 0.1 dynamic_slice.14
  34.7 20.7 %all-reduce.6.cloned.1.call-done = bf16[32,2056]{1,0:T(8,128)(2,1)} async-done(((bf16[32,2056]{1,0:T(8,128)(2,1)}), bf16[32,2056]{1,0:T(8,128)(2,1)}) %all-reduce.6.cloned.1.call-update) | async-done | bytes 131600
  55.4 0.8 convert_multiply_fusion.1
  56.2 0.1 multiply_reduce_fusion
  56.3 0.1 fusion.23
  56.4 0.1 copy.33
  56.5 0.1 copy.34
  56.6 0.1 multiply_bitcast_fusion
  56.7 3.6 %fusion.16 = f32[8,4,1,128]{3,2,1,0:T(1,128)S(1)} fusion(f32[8,4,128,128]{3,2,1,0:T(8,128)} %param.17, f32[8,4,128,1]{2,0,1,3:T(8,128)S(1)} %bitcast.70), kind=kOutput, calls=%fused_computation.43 | convolution fusion | flops 6291456 | bytes 2129920 | tf_op jit(solution)/shard_map/bhkv,bhk->bhv/dot_general | solution.py:28
  60.2 0.1 fusion.13
  60.3 0.8 multiply_add_fusion
  61.1 0.0 copy-start.2
  61.1 0.0 copy-start.7
  61.1 0.0 copy-start.4
  61.1 0.0 copy-start.8
  61.1 1.3 copy-done.2
  62.4 1.9 %fusion.14 = f32[8,4,1,128]{3,2,1,0:T(1,128)S(1)} fusion(f32[8,4,128,128]{3,2,1,0:T(8,128)S(1)} %multiply_add_fusion, f32[8,4,128,1]{2,0,1,3:T(8,128)S(1)} %get-tuple-element.4), kind=kOutput, calls=%fused_computation.41 | convolution fusion | flops 6291456 | bytes 2129920 | tf_op jit(solution)/shard_map/bhkv,bhk->bhv/dot_general | solution.py:33
  64.3 0.1 fusion.8
  64.4 0.1 fusion.18
  64.5 13.1 %all_gather.17 = bf16[32,512]{1,0:T(8,128)(2,1)S(1)} all-gather(bf16[8,512]{1,0:T(8,128)(2,1)S(1)} %fusion.18), channel_id=1, replica_groups=mesh['dp'=4,'kv'=4,'tp'=2] {'kv'}, dimensions={0}, use_global_device_ids=true | all-gather | bytes 40960 | tf_op jit(solution)/shard_map/all_gather | solution.py:103
  77.6 0.8 convolution_convert_fusion.3
  78.4 0.0 reduce-scatter.3.cloned.1.call-update
  78.5 0.0 all-reduce.4.cloned.1.call-start
  78.5 0.0 copy-done.8
  78.5 0.1 dynamic-slice_convert_fusion
  78.6 7.6 %reduce-scatter.3.cloned.1.call-done = bf16[32,256]{1,0:T(8,128)(2,1)} async-done(((bf16[32,512]{1,0:T(8,128)(2,1)}), bf16[32,256]{1,0:T(8,128)(2,1)}) %reduce-scatter.3.cloned.1.call-update) | async-done | bytes 16400 | tf_op jit(solution)/shard_map/reduce_scatter | solution.py:105
  86.2 0.8 fusion.6
  87.0 11.1 %all-gather.1 = bf16[4,1,32]{2,1,0:T(2,128)(2,1)S(1)} all-gather(bf16[1,1,32]{2,1,0:T(2,128)(2,1)S(1)} %bitcast.71), channel_id=1, replica_groups=mesh['dp'=4,'kv'=4,'tp'=2] {'kv'}, dimensions={0}, use_global_device_ids=true | all-gather | bytes 320 | tf_op jit(solution)/shard_map/all_gather | solution.py:115
  98.1 2.5 %psum.23 = f32[32]{0:T(128)S(1)} all-reduce(f32[32]{0:T(128)S(1)} %convert_reduce_fusion), channel_id=1, replica_groups=mesh['dp'=4,'kv'=4,'tp'=2] {'tp'}, use_global_device_ids=true, to_apply=%region_11.12 | all-reduce | flops 32 | bytes 256 | tf_op jit(solution)/shard_map/psum | solution.py:119
  100.6 13.2 %all_gather.18 = bf16[32,1024]{1,0:T(8,128)(2,1)S(1)} all-gather(bf16[32,256]{1,0:T(8,128)(2,1)S(1)} %get-tuple-element.9), channel_id=1, replica_groups=mesh['dp'=4,'kv'=4,'tp'=2] {'kv'}, dimensions={1}, use_global_device_ids=true | all-gather | bytes 81920 | tf_op jit(solution)/shard_map/all_gather | solution.py:114
  113.8 0.0 copy-done
  113.8 0.6 convolution_convert_fusion
  114.4 0.6 convolution_convert_fusion.1
  115.0 0.0 copy-start.6
  115.0 0.7 pad_maximum_fusion
  115.7 0.0 all-reduce.4.cloned.1.call-update
  115.7 0.0 reduce-scatter.5.cloned.1.call-start
  115.8 16.3 %all-reduce.4.cloned.1.call-done = bf16[32,2816]{1,0:T(8,128)(2,1)} async-done(((bf16[32,2816]{1,0:T(8,128)(2,1)}), bf16[32,2816]{1,0:T(8,128)(2,1)}) %all-reduce.4.cloned.1.call-update) | async-done | bytes 180240 | tf_op jit(solution)/shard_map/psum | solution.py:130
  132.1 1.0 convert_multiply_fusion
  133.1 3.0 %convolution_convert_fusion.2 = bf16[32,1024]{1,0:T(8,128)(2,1)} fusion(bf16[1408,1024]{1,0:T(8,128)(2,1)} %param.31, f32[32,2816]{1,0:T(8,128)S(1)} %convert_multiply_fusion), kind=kOutput, calls=%fused_computation.3 | convolution fusion | flops 92577792 | bytes 3309568 | tf_op jit(solution)/shard_map/dot_general | solution.py:135
  136.2 0.0 reduce-scatter.5.cloned.1.call-update
  136.2 20.7 %reduce-scatter.5.cloned.1.call-done = bf16[32,256]{1,0:T(8,128)(2,1)} async-done(((bf16[32,1024]{1,0:T(8,128)(2,1)}), bf16[32,256]{1,0:T(8,128)(2,1)}) %reduce-scatter.5.cloned.1.call-update) | async-done | bytes 16400 | tf_op jit(solution)/shard_map/reduce_scatter | solution.py:136
  156.8 1.3 fusion.7
  (20 shorter events, 0.1 us)
Async XLA Ops:
  7.2 106.7 %copy-start = (bf16[1024,1408]{1,0:T(8,128)(2,1)S(1)}, bf16[1024,1408]{1,0:T(8,128)(2,1)}, u32[]{:S(2)}) copy-start(bf16[1024,1408]{1,0:T(8,128)(2,1)} %param.30) | copy-start | bytes 8650756
  7.2 26.2 %copy-start.10 = (u32[32]{0:T(128)S(1)}, u32[32]{0:T(128)}, u32[]{:S(2)}) copy-start(u32[32]{0:T(128)} %constant.48) | copy-start | bytes 388
  7.2 10.9 %copy-start.5 = (bf16[32,256]{1,0:T(8,128)(2,1)S(1)}, bf16[32,256]{1,0:T(8,128)(2,1)}, u32[]{:S(2)}) copy-start(bf16[32,256]{1,0:T(8,128)(2,1)} %param.16) | copy-start | bytes 49156
  7.2 11.0 %copy-start.9 = (f32[4]{0:T(128)S(1)}, f32[4]{0:T(128)}, u32[]{:S(2)}) copy-start(f32[4]{0:T(128)} %param.25) | copy-start | bytes 52
  7.2 48.2 %all-reduce.6.cloned.1.call-start = ((), (), s32[]{:S(2)}) async-start(), calls=%async_computation.5 | async-start | bytes 278528
  18.0 68.2 %reduce-scatter.3.cloned.1.call-start = ((), (), s32[]{:S(2)}) async-start(), calls=%async_computation.2 | async-start | bytes 49152 | tf_op jit(solution)/shard_map/reduce_scatter | solution.py:105
  56.6 3.8 %copy-start.1 = (f32[8,4,128,128]{3,2,1,0:T(8,128)S(1)}, f32[8,4,128,128]{3,2,1,0:T(8,128)}, u32[]{:S(2)}) copy-start(f32[8,4,128,128]{3,2,1,0:T(8,128)} %param.17) | copy-start | bytes 6291460
  61.1 1.3 copy-start.2
  61.1 3.3 %copy-start.7 = (f32[128]{0:T(128)S(1)}, f32[128]{0:T(128)}, u32[]{:S(2)}) copy-start(f32[128]{0:T(128)} %param.26) | copy-start | bytes 1540
  61.1 16.5 %copy-start.4 = (bf16[512,512]{1,0:T(8,128)(2,1)S(1)}, bf16[512,512]{1,0:T(8,128)(2,1)}, u32[]{:S(2)}) copy-start(bf16[512,512]{1,0:T(8,128)(2,1)} %param.27) | copy-start | bytes 1572868
  61.1 17.4 %copy-start.8 = (bf16[512]{0:T(512)(128)(2,1)S(1)}, bf16[512]{0:T(512)(128)(2,1)}, u32[]{:S(2)}) copy-start(bf16[512]{0:T(512)(128)(2,1)} %param.28) | copy-start | bytes 3076
  78.5 53.7 %all-reduce.4.cloned.1.call-start = ((), (), s32[]{:S(2)}) async-start(), calls=%async_computation.3 | async-start | bytes 360448 | tf_op jit(solution)/shard_map/psum | solution.py:130
  100.6 13.8 %copy-start.3 = (bf16[1024,1408]{1,0:T(8,128)(2,1)S(1)}, bf16[1024,1408]{1,0:T(8,128)(2,1)}, u32[]{:S(2)}) copy-start(bf16[1024,1408]{1,0:T(8,128)(2,1)} %param.29) | copy-start | bytes 8650756
  115.0 41.8 %copy-start.6 = (bf16[32,256]{1,0:T(8,128)(2,1)S(1)}, bf16[32,256]{1,0:T(8,128)(2,1)}, u32[]{:S(2)}) copy-start(bf16[32,256]{1,0:T(8,128)(2,1)} %reduce-scatter.3.cloned.1.call-done) | copy-start | bytes 49156
  115.7 41.1 %reduce-scatter.5.cloned.1.call-start = ((), (), s32[]{:S(2)}) async-start(), calls=%async_computation.4 | async-start | bytes 81920 | tf_op jit(solution)/shard_map/reduce_scatter | solution.py:136
Sparse Core Ops, SparseCore 0:
  18.1 37.2 all-reduce.5
  78.6 7.5 reduce-scatter.2
  115.9 16.1 all-reduce.3
  136.3 20.4 reduce-scatter.4
where the time goes:
time: 165 us
  waiting for transfers between devices  65.3 us (40%)
  blocking collectives  57.3 us (35%)
  matrix products  17 us (10%)
  between operations  14.6 us (9%)
  other arithmetic  7.06 us (4%)
  local copies, waits for them, and re-layouts  3.14 us (2%)
    unnamed x5, waiting for transfers between devices  20.8 us
    reduce_scatter x1, waiting for transfers between devices, local(): lax.psum_scatter(down_local.astype(jnp.bfloat16), 'kv', scatter_dimension...  20.7 us
    psum x1, waiting for transfers between devices, local(): gate_up = lax.psum(summand.astype(jnp.bfloat16), 'tp').astype(jnp.float32)  16.3 us
    psum x1, blocking collectives, local(): square_total = lax.psum(jnp.sum(square_pair, axis=1), 'kv')  13.3 us
    all_gather x1, blocking collectives, local(): lax.all_gather(normed_own, 'kv', axis=1, tiled=True)  13.2 us
    all_gather x1, blocking collectives, local(): lax.all_gather(mixed, 'kv', axis=0, tiled=True)  13.1 us
    all_gather x1, blocking collectives, local(): lax.all_gather(mid_squares.astype(jnp.bfloat16), 'kv', axis=1, tiled=True)  11.1 us
    reduce_scatter x1, waiting for transfers between devices, local(): lax.psum_scatter(attn_part.astype(jnp.bfloat16), 'tp', scatter_dimension=...  7.59 us
  transfers between devices with their start and end apart: 4, of which 4 were waited for; matrix products, arithmetic and copies ran while one was open for 1% of the time, Pallas kernels for 0%

commit v1 on v0

--- a/solution.py
+++ b/solution.py
@@ -1,6 +1,9 @@
+import functools
 import jax
 import jax.numpy as jnp
 from jax import lax
+from jax.experimental import pallas as pl
+from jax.experimental.pallas import tpu as pltpu
 from jax.sharding import PartitionSpec as P
 
 D = 2048
@@ -140,6 +143,514 @@
     return (layer_out, next_state)
 
 
+F32 = jnp.float32
+BF16 = jnp.bfloat16
+MESH = pl.DeviceIdType.MESH
+
+
+def layer_kernel(
+    G,
+    decay_rate,
+    head_gain,
+    gain_in,
+    gain_mid,
+    tokens,
+    delta_state,
+    w_query,
+    w_key,
+    w_value,
+    w_out_gate,
+    w_beta,
+    w_decay,
+    w_mix,
+    w_gate,
+    w_up,
+    w_down,
+    layer_out,
+    next_state,
+    tok,
+    state,
+    wq,
+    wk,
+    wv,
+    wg,
+    wb,
+    wd,
+    wm,
+    wgate,
+    wup,
+    wdown,
+    part,
+    proj_out,
+    proj_in,
+    extra_out,
+    extra_in,
+    gain_out,
+    gain_all,
+    col_k,
+    col_q,
+    vec,
+    mixed_all,
+    attn_out,
+    attn_in,
+    mid_all,
+    middle,
+    acc,
+    gu_out,
+    gu_in,
+    sq_out,
+    sq_in,
+    down_out,
+    down_in,
+    out_buf,
+    load_sem,
+    tok_sem,
+    gain_sem,
+    proj_sem,
+    extra_sem,
+    mixed_sem,
+    attn_sem,
+    mid_sem,
+    gu_sem,
+    sq_sem,
+    down_sem,
+    store_sem,
+):
+    k = lax.axis_index("kv")
+    t = lax.axis_index("tp")
+    other = 1 - t
+    R, F = tokens.shape
+    own = R // G
+    C = w_query.shape[1]
+    H = C // HEAD_DIM
+    HEADS = w_beta.shape[1]
+    HID = w_gate.shape[1]
+    partner = {"tp": other}
+    offsets = sorted(range(1, G), key=lambda d: -min(d, G - d))
+
+    def peer(d):
+        return lax.rem(k + d, G)
+
+    def source(d):
+        return lax.rem(k + G - d, G)
+
+    loads = []
+
+    def load(src, dst):
+        copy = pltpu.make_async_copy(src, dst, load_sem.at[len(loads)])
+        copy.start()
+        loads.append(copy)
+        return copy
+
+    def remote(src, dst, sems, slot_send, slot_recv, device):
+        return pltpu.make_async_remote_copy(
+            src_ref=src,
+            dst_ref=dst,
+            send_sem=sems.at[0, slot_send],
+            recv_sem=sems.at[1, slot_recv],
+            device_id=device,
+            device_id_type=MESH,
+        )
+
+    load_tok = load(tokens, tok.at[t])
+    barrier = pltpu.get_barrier_semaphore()
+    pl.semaphore_signal(barrier, inc=1, device_id=partner, device_id_type=MESH)
+    for d in offsets:
+        pl.semaphore_signal(barrier, inc=1, device_id={"kv": peer(d)}, device_id_type=MESH)
+    load_proj = [
+        load(a, b)
+        for a, b in (
+            (w_query, wq),
+            (w_key, wk),
+            (w_value, wv),
+            (w_out_gate, wg),
+            (w_beta, wb),
+            (w_decay, wd),
+        )
+    ]
+    load_state = load(delta_state, state)
+    load_mix = load(w_mix, wm)
+    load_gate = load(w_gate, wgate)
+    load_up = load(w_up, wup)
+    load_down = load(w_down, wdown)
+
+    gain_mid_own = gain_mid[:, pl.ds(pl.multiple_of(t * F, F), F)].astype(F32)
+    gain_out[...] = jnp.broadcast_to(gain_mid_own, gain_out.shape)
+    gain_all[k] = jnp.broadcast_to(gain_mid_own, gain_out.shape)
+    load_tok.wait()
+    pl.semaphore_wait(barrier, G)
+
+    send_tok = remote(tok.at[t], tok.at[t], tok_sem, 0, 0, partner)
+    send_tok.start()
+    gain_copies = []
+    for d in offsets:
+        copy = remote(gain_out, gain_all.at[k], gain_sem, d - 1, d - 1, {"kv": peer(d)})
+        copy.start()
+        gain_copies.append((d, copy))
+
+    weights = (wq, wk, wv, wg)
+
+    def rows_of(half):
+        return pl.ds(pl.multiple_of(half * F, F), F)
+
+    def scaled(half):
+        x = tok[half].astype(F32)
+        gain = gain_in[:, rows_of(half)].astype(F32)
+        return (x * gain).astype(BF16), jnp.sum(x * x, axis=1, keepdims=True)
+
+    x_own, sq_own = scaled(t)
+    for copy, i in zip(load_proj, range(6)):
+        copy.wait()
+        if i < 4:
+            part[:, i * C : (i + 1) * C] = jnp.dot(
+                x_own, weights[i][rows_of(t), :], preferred_element_type=F32
+            )
+    beta_own = jnp.dot(x_own, wb[rows_of(t), :], preferred_element_type=F32)
+    decay_own = jnp.dot(x_own, wd[rows_of(t), :], preferred_element_type=F32)
+
+    remote(tok.at[t], tok.at[other], tok_sem, 0, 0, partner).wait_recv()
+    x_two, sq_two = scaled(other)
+    extra = jnp.zeros((R, 128), F32)
+    extra_out[...] = extra.reshape(G, own, 128)
+    beta = beta_own + jnp.dot(x_two, wb[rows_of(other), :], preferred_element_type=F32)
+    decay = decay_own + jnp.dot(x_two, wd[rows_of(other), :], preferred_element_type=F32)
+    extra_out[:, :, 0:HEADS] = beta.reshape(G, own, HEADS)
+    extra_out[:, :, HEADS : 2 * HEADS] = decay.reshape(G, own, HEADS)
+    extra_out[:, :, 2 * HEADS : 2 * HEADS + 1] = (sq_own + sq_two).reshape(G, own, 1)
+    proj_copies = []
+    for chunk in range(2):
+        for j in range(2):
+            i = 2 * chunk + j
+            cols = slice(i * C, (i + 1) * C)
+            value = part[:, cols] + jnp.dot(
+                x_two, weights[i][rows_of(other), :], preferred_element_type=F32
+            )
+            part[:, cols] = value
+            proj_out[chunk, :, :, j * C : (j + 1) * C] = value.astype(BF16).reshape(G, own, C)
+        for d in offsets:
+            copy = remote(
+                proj_out.at[chunk, peer(d)],
+                proj_in.at[chunk, d - 1],
+                proj_sem,
+                chunk * (G - 1) + d - 1,
+                chunk * (G - 1) + d - 1,
+                {"kv": peer(d)},
+            )
+            copy.start()
+            proj_copies.append(copy)
+            if chunk == 0:
+                copy = remote(
+                    extra_out.at[peer(d)], extra_in.at[d - 1], extra_sem, d - 1, d - 1, {"kv": peer(d)}
+                )
+                copy.start()
+                proj_copies.append(copy)
+    own_rows = pl.ds(pl.multiple_of(k * own, own), own)
+    sum_extra = extra_out[k]
+    for d in range(1, G):
+        remote(extra_out.at[0], extra_in.at[d - 1], extra_sem, d - 1, d - 1, partner).wait_recv()
+        sum_extra = sum_extra + extra_in[d - 1]
+    lane = lax.broadcasted_iota(jnp.int32, (own, 128), 1)
+
+    def lane_of(column):
+        return jnp.sum(jnp.where(lane == column, sum_extra, 0.0), axis=1, keepdims=True)
+
+    row_scale = lax.rsqrt(lane_of(2 * HEADS) / D + norm_epsilon)
+
+    def chunk_sum(chunk):
+        total = part[own_rows, 2 * chunk * C : 2 * (chunk + 1) * C]
+        for d in range(1, G):
+            remote(
+                proj_out.at[chunk, 0],
+                proj_in.at[chunk, d - 1],
+                proj_sem,
+                chunk * (G - 1) + d - 1,
+                chunk * (G - 1) + d - 1,
+                partner,
+            ).wait_recv()
+            total = total + proj_in[chunk, d - 1].astype(F32)
+        return total * row_scale
+
+    query_key = chunk_sum(0)
+    for h in range(H):
+        cols = slice(h * HEAD_DIM, (h + 1) * HEAD_DIM)
+        query = unit_rows(jax.nn.silu(query_key[:, cols])) * HEAD_DIM ** (-0.5)
+        key_vec = unit_rows(jax.nn.silu(query_key[:, C + h * HEAD_DIM : C + (h + 1) * HEAD_DIM]))
+        col_q[h] = query.T
+        col_k[h] = key_vec.T
+        vec[0, h] = jnp.broadcast_to(
+            jnp.sum(query * key_vec, axis=1, keepdims=True), (own, HEAD_DIM)
+        )
+        vec[1, h] = jnp.broadcast_to(jax.nn.sigmoid(lane_of(t * H + h) * row_scale), (own, HEAD_DIM))
+        pre = lane_of(HEADS + t * H + h) * row_scale
+        softplus = jnp.maximum(pre, 0.0) + jnp.log1p(jnp.exp(-jnp.abs(pre)))
+        vec[2, h] = jnp.broadcast_to(jnp.exp(-decay_rate[h] * softplus), (own, HEAD_DIM))
+    load_state.wait()
+
+    def recall(h, carry):
+        kc, qc = col_k[h], col_q[h]
+        recalled, asked = [], []
+        for s in range(own):
+            block = state[s, h]
+            recalled.append(jnp.sum(block * kc[:, s : s + 1], axis=0, keepdims=True))
+            asked.append(jnp.sum(block * qc[:, s : s + 1], axis=0, keepdims=True))
+        vec[3, h] = jnp.concatenate(recalled, axis=0)
+        vec[4, h] = jnp.concatenate(asked, axis=0)
+        return carry
+
+    lax.fori_loop(0, H, recall, 0)
+    value_gate = chunk_sum(1)
+    gain_row = head_gain[...]
+    for h in range(H):
+        cols = slice(h * HEAD_DIM, (h + 1) * HEAD_DIM)
+        value_vec = jax.nn.silu(value_gate[:, cols])
+        gate = jax.nn.silu(value_gate[:, C + h * HEAD_DIM : C + (h + 1) * HEAD_DIM])
+        keep = vec[2, h]
+        correction = vec[1, h] * (value_vec - keep * vec[3, h])
+        readout = keep * vec[4, h] + vec[0, h] * correction
+        vec[3, h] = correction
+        readout = readout * lax.rsqrt(
+            jnp.mean(readout * readout, axis=-1, keepdims=True) + norm_epsilon
+        )
+        mixed_all[k, :, cols] = (readout * gain_row * gate).astype(BF16)
+    mixed_copies = []
+    for d in offsets:
+        copy = remote(
+            mixed_all.at[k], mixed_all.at[k], mixed_sem, d - 1, d - 1, {"kv": peer(d)}
+        )
+        copy.start()
+        mixed_copies.append(copy)
+
+    def update(h, carry):
+        kc = col_k[h]
+        keep, correction = vec[2, h], vec[3, h]
+        for s in range(own):
+            state[s, h] = (
+                keep[s : s + 1] * state[s, h] + kc[:, s : s + 1] * correction[s : s + 1]
+            )
+        return carry
+
+    lax.fori_loop(0, H, update, 0)
+    load_mix.wait()
+    for d in range(1, G):
+        remote(
+            mixed_all.at[k], mixed_all.at[source(d)], mixed_sem, d - 1, d - 1, partner
+        ).wait_recv()
+    store_state = pltpu.make_async_copy(state, next_state, store_sem.at[0])
+    store_state.start()
+    mixed = jnp.concatenate([mixed_all[j].astype(F32) for j in range(G)], axis=0).astype(BF16)
+    attn_out[...] = jnp.dot(
+        mixed, wm[:, pl.ds(pl.multiple_of(other * F, F), F)], preferred_element_type=F32
+    ).astype(BF16)
+    send_attn = remote(attn_out, attn_in, attn_sem, 0, 0, partner)
+    send_attn.start()
+    attn = jnp.dot(
+        mixed, wm[:, pl.ds(pl.multiple_of(t * F, F), F)], preferred_element_type=F32
+    ).astype(BF16)
+    send_attn.wait_recv()
+    mid = (tok[t].astype(F32) + (attn.astype(F32) + attn_in[...].astype(F32))).astype(BF16)
+    middle[...] = mid
+    mid_all[k] = mid
+    mid_copies = []
+    for d in offsets:
+        copy = remote(middle, mid_all.at[k], mid_sem, d - 1, d - 1, {"kv": peer(d)})
+        copy.start()
+        mid_copies.append(copy)
+
+    cut = (HID // 128 + 1) // 2 * 128
+    spans = (slice(0, cut), slice(cut, HID))
+    squares = jnp.zeros((R, 1), F32)
+    load_gate.wait()
+    load_up.wait()
+    for d, copy in gain_copies:
+        remote(gain_out, gain_all.at[source(d)], gain_sem, d - 1, d - 1, partner).wait_recv()
+    order = [0] + sorted(range(1, G), key=lambda d: min(d, G - d))
+    gu_copies = []
+    for position, d in enumerate(order):
+        src = source(d) if d else k
+        if d:
+            remote(middle, mid_all.at[src], mid_sem, d - 1, d - 1, partner).wait_recv()
+        x = mid_all[src].astype(F32)
+        squares = squares + jnp.sum(x * x, axis=1, keepdims=True)
+        x = (x * gain_all[src][0:1]).astype(BF16)
+        rows = pl.ds(pl.multiple_of(src * F, F), F)
+        last = position == G - 1
+        if last:
+            sq_out[...] = jnp.broadcast_to(squares, sq_out.shape)
+            send_sq = remote(sq_out, sq_in, sq_sem, 0, 0, partner)
+            send_sq.start()
+        for c, span in enumerate(spans):
+            for j, w in enumerate((wgate, wup)):
+                value = jnp.dot(x, w[rows, span], preferred_element_type=F32)
+                if position:
+                    value = acc[j, :, span] + value
+                acc[j, :, span] = value
+                if last:
+                    gu_out[j, :, span] = value.astype(BF16)
+            if last:
+                copy = remote(
+                    gu_out.at[:, :, span], gu_in.at[:, :, span], gu_sem, c, c, partner
+                )
+                copy.start()
+                gu_copies.append(copy)
+    send_sq.wait_recv()
+    mid_scale = lax.rsqrt((squares + sq_in[:, 0:1]) / D + norm_epsilon)
+    pieces = []
+    for c, span in enumerate(spans):
+        gu_copies[c].wait_recv()
+        gate = (acc[0, :, span] + gu_in[0, :, span].astype(F32)) * mid_scale
+        up = (acc[1, :, span] + gu_in[1, :, span].astype(F32)) * mid_scale
+        pieces.append((jax.nn.silu(gate) * up).astype(BF16))
+    load_down.wait()
+    down_copies = []
+    for d in offsets + [0]:
+        dst = peer(d) if d else k
+        cols = pl.ds(pl.multiple_of(dst * F, F), F)
+        value = sum(
+            jnp.dot(piece, wdown[span, cols], preferred_element_type=F32)
+            for piece, span in zip(pieces, spans)
+        )
+        if d:
+            down_out[d - 1] = value.astype(BF16)
+            copy = remote(
+                down_out.at[d - 1], down_in.at[d - 1], down_sem, d - 1, d - 1, {"kv": dst}
+            )
+            copy.start()
+            down_copies.append(copy)
+    total = value
+    for d in sorted(range(1, G), key=lambda d: min(d, G - d)):
+        remote(down_out.at[d - 1], down_in.at[d - 1], down_sem, d - 1, d - 1, partner).wait_recv()
+        total = total + down_in[d - 1].astype(F32)
+    out_buf[...] = (middle[...].astype(F32) + total).astype(BF16)
+    store_out = pltpu.make_async_copy(out_buf, layer_out, store_sem.at[1])
+    store_out.start()
+    send_tok.wait_send()
+    for d, copy in gain_copies:
+        copy.wait_send()
+    for copy in proj_copies + mixed_copies + mid_copies + gu_copies + down_copies:
+        copy.wait_send()
+    send_attn.wait_send()
+    send_sq.wait_send()
+    store_state.wait()
+    store_out.wait()
+
+
+def one_kernel(
+    tokens,
+    delta_state,
+    gain_in,
+    w_query,
+    w_key,
+    w_value,
+    w_out_gate,
+    w_beta,
+    w_decay,
+    decay_rate,
+    head_gain,
+    w_mix,
+    gain_mid,
+    w_gate,
+    w_up,
+    w_down,
+):
+    G = lax.axis_size("kv")
+    R, F = tokens.shape
+    own = R // G
+    C = w_query.shape[1]
+    H = C // HEAD_DIM
+    HID = w_gate.shape[1]
+    vmem = lambda like: pltpu.VMEM(like.shape, like.dtype)
+    dma = pltpu.SemaphoreType.DMA
+    anywhere = pl.BlockSpec(memory_space=pl.ANY)
+    inside = pl.BlockSpec(memory_space=pltpu.VMEM)
+    return pl.pallas_call(
+        functools.partial(layer_kernel, G),
+        out_shape=(
+            jax.ShapeDtypeStruct(tokens.shape, BF16),
+            jax.ShapeDtypeStruct(delta_state.shape, F32),
+        ),
+        in_specs=[pl.BlockSpec(memory_space=pltpu.SMEM)] + [inside] * 3 + [anywhere] * 12,
+        out_specs=(anywhere, anywhere),
+        scratch_shapes=[
+            pltpu.VMEM((2, R, F), BF16),
+            vmem(delta_state),
+            vmem(w_query),
+            vmem(w_key),
+            vmem(w_value),
+            vmem(w_out_gate),
+            vmem(w_beta),
+            vmem(w_decay),
+            vmem(w_mix),
+            vmem(w_gate),
+            vmem(w_up),
+            vmem(w_down),
+            pltpu.VMEM((R, 4 * C), F32),
+            pltpu.VMEM((2, G, own, 2 * C), BF16),
+            pltpu.VMEM((2, G - 1, own, 2 * C), BF16),
+            pltpu.VMEM((G, own, 128), F32),
+            pltpu.VMEM((G - 1, own, 128), F32),
+            pltpu.VMEM((8, F), F32),
+            pltpu.VMEM((G, 8, F), F32),
+            pltpu.VMEM((H, HEAD_DIM, own), F32),
+            pltpu.VMEM((H, HEAD_DIM, own), F32),
+            pltpu.VMEM((5, H, own, HEAD_DIM), F32),
+            pltpu.VMEM((G, own, C), BF16),
+            pltpu.VMEM((R, F), BF16),
+            pltpu.VMEM((R, F), BF16),
+            pltpu.VMEM((G, R, F), BF16),
+            pltpu.VMEM((R, F), BF16),
+            pltpu.VMEM((2, R, HID), F32),
+            pltpu.VMEM((2, R, HID), BF16),
+            pltpu.VMEM((2, R, HID), BF16),
+            pltpu.VMEM((R, 128), F32),
+            pltpu.VMEM((R, 128), F32),
+            pltpu.VMEM((G - 1, R, F), BF16),
+            pltpu.VMEM((G - 1, R, F), BF16),
+            pltpu.VMEM((R, F), BF16),
+            dma((12,)),
+            dma((2, 1)),
+            dma((2, G - 1)),
+            dma((2, 2 * (G - 1))),
+            dma((2, G - 1)),
+            dma((2, G - 1)),
+            dma((2, 1)),
+            dma((2, G - 1)),
+            dma((2, 2)),
+            dma((2, 1)),
+            dma((2, G - 1)),
+            dma((2,)),
+        ],
+        compiler_params=pltpu.CompilerParams(
+            collective_id=0, has_side_effects=True, vmem_limit_bytes=60 * 2**20
+        ),
+    )(
+        decay_rate,
+        head_gain.reshape(1, -1),
+        gain_in.reshape(1, -1),
+        gain_mid.reshape(1, -1),
+        tokens,
+        delta_state,
+        w_query,
+        w_key,
+        w_value,
+        w_out_gate,
+        w_beta,
+        w_decay,
+        w_mix,
+        w_gate,
+        w_up,
+        w_down,
+    )
+
+
+def step(*args):
+    tokens, w_query, w_gate = args[0], args[3], args[13]
+    rows, features = tokens.shape
+    aligned = features % 128 == 0 and w_gate.shape[1] % 128 == 0
+    aligned = aligned and w_query.shape[1] % HEAD_DIM == 0 and w_query.shape[0] == 2 * features
+    aligned = aligned and rows % (8 * lax.axis_size("kv")) == 0 and lax.axis_size("tp") == 2
+    return one_kernel(*args) if aligned else local(*args)
+
+
 def solution(mesh):
     in_specs = (
         P("dp", ("kv", "tp")),
@@ -160,4 +671,4 @@
         P("kv", "tp"),
     )
     out_specs = (P("dp", ("kv", "tp")), P(("dp", "kv"), "tp", None, None))
-    return jax.shard_map(local, mesh=mesh, in_specs=in_specs, out_specs=out_specs, check_vma=False)
+    return jax.shard_map(step, mesh=mesh, in_specs=in_specs, out_specs=out_specs, check_vma=False)

time: 165 us -> 40 us (0.24)
  waiting for transfers between devices: 65.3 us -> 0 us
  blocking collectives: 57.3 us -> 0 us
  Pallas kernels: 0 us -> 28.9 us
  matrix products: 17 us -> 0 us
  between operations: 14.6 us -> 0.64 us
  other arithmetic: 7.06 us -> 0 us
  local copies, waits for them, and re-layouts: 3.14 us -> 9.98 us
    all_gather x5 -> x0, blocking collectives: 41.6 us -> none  [the longest x1 13.2 us: local(): lax.all_gather(normed_own, 'kv', axis=1, tiled=True)]
    pallas_call x0 -> x1, Pallas kernels: none -> 28.9 us  [one_kernel(): pl.pallas_call(functools.partial(layer_kernel, G), out_shape=(jax.ShapeDt...]
    reduce_scatter x2 -> x0, waiting for transfers between devices: 28.3 us -> none  [the longest x1 20.7 us: local(): lax.psum_scatter(down_local.astype(jnp.bfloat16), 'kv', scatter_dimension...]
    unnamed x5 -> x0, waiting for transfers between devices: 20.8 us -> none
    dot_general x12 -> x0, matrix products: 17 us -> none  [the longest x6 6.6 us: local(): jnp.dot(row_block, weight, preferred_element_type=jnp.float32)]
    psum x1 -> x0, waiting for transfers between devices: 16.3 us -> none  [local(): gate_up = lax.psum(summand.astype(jnp.bfloat16), 'tp').astype(jnp.float32)]
    psum x2 -> x0, blocking collectives: 15.8 us -> none  [the longest x1 13.3 us: local(): square_total = lax.psum(jnp.sum(square_pair, axis=1), 'kv')]
    unnamed x23 -> x4, local copies, waits for them, and re-layouts: 1.92 us -> 7.45 us
  transfers between devices with their start and end apart: 4 -> 0, of which waited for: 4 -> 0; matrix products, arithmetic and copies ran while one was open for 1% -> 0% of each run, Pallas kernels for 0% -> 0%
where the time goes in v1:
time: 40 us; the launch traced here: 39.5 us
  Pallas kernels  28.9 us (72%)
  local copies, waits for them, and re-layouts  9.98 us (25%)
  between operations  0.64 us (2%)
    pallas_call x1, Pallas kernels, one_kernel(): pl.pallas_call(functools.partial(layer_kernel, G), out_shape=(jax.ShapeDt...  28.9 us
    unnamed x4, local copies, waits for them, and re-layouts  7.45 us
    reshape x1, local copies, waits for them, and re-layouts, one_kernel(): gain_mid.reshape(1, -1)  1.27 us
    reshape x1, local copies, waits for them, and re-layouts, one_kernel(): gain_in.reshape(1, -1)  1.26 us

profile of v1, /device:TPU:0, one launch (start us, length us, event | category | flops | bytes accessed | tf_op | source)
XLA Modules:
  0.0 39.5 jit_solution(10905749085880866140)
XLA Ops:
  0.6 1.3 %reshape.14.gain_in = bf16[1,512]{1,0:T(2,128)(2,1)} reshape(bf16[512]{0:T(512)(128)(2,1)} %param.18) | data formatting | bytes 2048 | tf_op jit(solution)/shard_map/reshape | solution.py:628
  1.9 1.3 %reshape.15.gain_mid = bf16[1,512]{1,0:T(2,128)(2,1)} reshape(bf16[512]{0:T(512)(128)(2,1)} %param.28) | data formatting | bytes 2048 | tf_op jit(solution)/shard_map/reshape | solution.py:629
  3.2 1.5 %copy.18.w_beta = bf16[512,8]{1,0:T(8,128)(2,1)} copy(bf16[512,8]{0,1:T(8,128)(2,1)} %param.23) | data formatting | bytes 16384 | tf_op args[7]
  4.7 1.5 %copy.19.w_decay = bf16[512,8]{1,0:T(8,128)(2,1)} copy(bf16[512,8]{0,1:T(8,128)(2,1)} %param.24) | data formatting | bytes 16384 | tf_op args[8]
  6.2 28.9 %shard_map.167 = (bf16[32,256]{1,0:T(8,128)(2,1)}, f32[8,4,128,128]{3,2,1,0:T(8,128)}) custom-call(f32[4]{0:T(128)} %decay_rate.1, f32[1,128]{1,0:T(1,128)} %bitcast.1, bf16[1,512]{1,0:T(2,128)(2,1)} %reshape.14.gain_in, bf16[1,512]{1,0:T(2,128)(2,1)} %reshape.15.gain_mid, bf16[32,256]{1,0:T(8,128)(2,1)} %tokens.1, f32[8,4,128,128]{3,2,1,0:T(8,128)} %delta_state.1, ...), custom_call_target="tpu_custom_call" | custom-call | tf_op jit(solution)/shard_map/pallas_call | solution.py:565
  35.0 1.3 %copy.22 = bf16[32,256]{1,0:T(8,128)(2,1)} copy(bf16[32,256]{1,0:T(8,128)(2,1)} %get-tuple-element.4) | data formatting | bytes 32768
  36.4 3.1 %copy.23 = f32[8,4,128,128]{3,2,1,0:T(8,128)} copy(f32[8,4,128,128]{3,2,1,0:T(8,128)} %get-tuple-element.5) | data formatting | bytes 4194304

commit v2 on v1

--- a/solution.py
+++ b/solution.py
@@ -146,6 +146,17 @@
 F32 = jnp.float32
 BF16 = jnp.bfloat16
 MESH = pl.DeviceIdType.MESH
+
+
+def by_column(left, right):
+    return lax.dot_general(
+        left, right, (((1,), (1,)), ((), ())), preferred_element_type=jnp.float32
+    )
+
+
+def as_row(matrix):
+    matrix = matrix.astype(jnp.float32)
+    return jnp.concatenate([matrix[i : i + 1] for i in range(matrix.shape[0])], axis=1)
 
 
 def layer_kernel(
@@ -202,7 +213,8 @@
     sq_in,
     down_out,
     down_in,
-    out_buf,
+    gain_row_in,
+    gain_row_mid,
     load_sem,
     tok_sem,
     gain_sem,
@@ -214,7 +226,6 @@
     gu_sem,
     sq_sem,
     down_sem,
-    store_sem,
 ):
     k = lax.axis_index("kv")
     t = lax.axis_index("tp")
@@ -223,16 +234,20 @@
     own = R // G
     C = w_query.shape[1]
     H = C // HEAD_DIM
-    HEADS = w_beta.shape[1]
+    HEADS = w_beta.shape[0]
     HID = w_gate.shape[1]
     partner = {"tp": other}
-    offsets = sorted(range(1, G), key=lambda d: -min(d, G - d))
-
-    def peer(d):
-        return lax.rem(k + d, G)
-
-    def source(d):
-        return lax.rem(k + G - d, G)
+    upper = lax.div(k, G // 2)
+
+    def above(a, b):
+        return lax.div(a - b + G - 1, G)
+
+    def far(j):
+        down = G - 1 - j
+        return (1 - upper) * (down - 1 + above(down, k)) + upper * (j + 1 - above(k, j))
+
+    others = [far(j) for j in range(G - 1)]
+    nearest = others[::-1]
 
     loads = []
 
@@ -255,8 +270,8 @@
     load_tok = load(tokens, tok.at[t])
     barrier = pltpu.get_barrier_semaphore()
     pl.semaphore_signal(barrier, inc=1, device_id=partner, device_id_type=MESH)
-    for d in offsets:
-        pl.semaphore_signal(barrier, inc=1, device_id={"kv": peer(d)}, device_id_type=MESH)
+    for dst in others:
+        pl.semaphore_signal(barrier, inc=1, device_id={"kv": dst}, device_id_type=MESH)
     load_proj = [
         load(a, b)
         for a, b in (
@@ -268,13 +283,10 @@
             (w_decay, wd),
         )
     ]
-    load_state = load(delta_state, state)
-    load_mix = load(w_mix, wm)
-    load_gate = load(w_gate, wgate)
-    load_up = load(w_up, wup)
-    load_down = load(w_down, wdown)
-
-    gain_mid_own = gain_mid[:, pl.ds(pl.multiple_of(t * F, F), F)].astype(F32)
+
+    gain_row_in[...] = as_row(gain_in[...])
+    gain_row_mid[...] = as_row(gain_mid[...])
+    gain_mid_own = gain_row_mid[:, pl.ds(pl.multiple_of(t * F, F), F)]
     gain_out[...] = jnp.broadcast_to(gain_mid_own, gain_out.shape)
     gain_all[k] = jnp.broadcast_to(gain_mid_own, gain_out.shape)
     load_tok.wait()
@@ -283,10 +295,10 @@
     send_tok = remote(tok.at[t], tok.at[t], tok_sem, 0, 0, partner)
     send_tok.start()
     gain_copies = []
-    for d in offsets:
-        copy = remote(gain_out, gain_all.at[k], gain_sem, d - 1, d - 1, {"kv": peer(d)})
+    for j, dst in enumerate(others):
+        copy = remote(gain_out, gain_all.at[k], gain_sem, j, k, {"kv": dst})
         copy.start()
-        gain_copies.append((d, copy))
+        gain_copies.append(copy)
 
     weights = (wq, wk, wv, wg)
 
@@ -295,7 +307,7 @@
 
     def scaled(half):
         x = tok[half].astype(F32)
-        gain = gain_in[:, rows_of(half)].astype(F32)
+        gain = gain_row_in[:, rows_of(half)]
         return (x * gain).astype(BF16), jnp.sum(x * x, axis=1, keepdims=True)
 
     x_own, sq_own = scaled(t)
@@ -305,15 +317,20 @@
             part[:, i * C : (i + 1) * C] = jnp.dot(
                 x_own, weights[i][rows_of(t), :], preferred_element_type=F32
             )
-    beta_own = jnp.dot(x_own, wb[rows_of(t), :], preferred_element_type=F32)
-    decay_own = jnp.dot(x_own, wd[rows_of(t), :], preferred_element_type=F32)
+    load_state = load(delta_state, state)
+    load_mix = load(w_mix, wm)
+    load_gate = load(w_gate, wgate)
+    load_up = load(w_up, wup)
+    load_down = load(w_down, wdown)
+    beta_own = by_column(x_own, wb[:, rows_of(t)])
+    decay_own = by_column(x_own, wd[:, rows_of(t)])
 
     remote(tok.at[t], tok.at[other], tok_sem, 0, 0, partner).wait_recv()
     x_two, sq_two = scaled(other)
     extra = jnp.zeros((R, 128), F32)
     extra_out[...] = extra.reshape(G, own, 128)
-    beta = beta_own + jnp.dot(x_two, wb[rows_of(other), :], preferred_element_type=F32)
-    decay = decay_own + jnp.dot(x_two, wd[rows_of(other), :], preferred_element_type=F32)
+    beta = beta_own + by_column(x_two, wb[:, rows_of(other)])
+    decay = decay_own + by_column(x_two, wd[:, rows_of(other)])
     extra_out[:, :, 0:HEADS] = beta.reshape(G, own, HEADS)
     extra_out[:, :, HEADS : 2 * HEADS] = decay.reshape(G, own, HEADS)
     extra_out[:, :, 2 * HEADS : 2 * HEADS + 1] = (sq_own + sq_two).reshape(G, own, 1)
@@ -327,28 +344,26 @@
             )
             part[:, cols] = value
             proj_out[chunk, :, :, j * C : (j + 1) * C] = value.astype(BF16).reshape(G, own, C)
-        for d in offsets:
+        for j, dst in enumerate(others):
             copy = remote(
-                proj_out.at[chunk, peer(d)],
-                proj_in.at[chunk, d - 1],
+                proj_out.at[chunk, dst],
+                proj_in.at[chunk, k],
                 proj_sem,
-                chunk * (G - 1) + d - 1,
-                chunk * (G - 1) + d - 1,
-                {"kv": peer(d)},
+                chunk * G + j,
+                chunk * G + k,
+                {"kv": dst},
             )
             copy.start()
             proj_copies.append(copy)
             if chunk == 0:
-                copy = remote(
-                    extra_out.at[peer(d)], extra_in.at[d - 1], extra_sem, d - 1, d - 1, {"kv": peer(d)}
-                )
+                copy = remote(extra_out.at[dst], extra_in.at[k], extra_sem, j, k, {"kv": dst})
                 copy.start()
                 proj_copies.append(copy)
     own_rows = pl.ds(pl.multiple_of(k * own, own), own)
     sum_extra = extra_out[k]
-    for d in range(1, G):
-        remote(extra_out.at[0], extra_in.at[d - 1], extra_sem, d - 1, d - 1, partner).wait_recv()
-        sum_extra = sum_extra + extra_in[d - 1]
+    for src in nearest:
+        remote(extra_out.at[0], extra_in.at[src], extra_sem, 0, src, partner).wait_recv()
+        sum_extra = sum_extra + extra_in[src]
     lane = lax.broadcasted_iota(jnp.int32, (own, 128), 1)
 
     def lane_of(column):
@@ -358,16 +373,16 @@
 
     def chunk_sum(chunk):
         total = part[own_rows, 2 * chunk * C : 2 * (chunk + 1) * C]
-        for d in range(1, G):
+        for src in nearest:
             remote(
                 proj_out.at[chunk, 0],
-                proj_in.at[chunk, d - 1],
+                proj_in.at[chunk, src],
                 proj_sem,
-                chunk * (G - 1) + d - 1,
-                chunk * (G - 1) + d - 1,
+                chunk * G,
+                chunk * G + src,
                 partner,
             ).wait_recv()
-            total = total + proj_in[chunk, d - 1].astype(F32)
+            total = total + proj_in[chunk, src].astype(F32)
         return total * row_scale
 
     query_key = chunk_sum(0)
@@ -413,10 +428,8 @@
         )
         mixed_all[k, :, cols] = (readout * gain_row * gate).astype(BF16)
     mixed_copies = []
-    for d in offsets:
-        copy = remote(
-            mixed_all.at[k], mixed_all.at[k], mixed_sem, d - 1, d - 1, {"kv": peer(d)}
-        )
+    for j, dst in enumerate(others):
+        copy = remote(mixed_all.at[k], mixed_all.at[k], mixed_sem, j, k, {"kv": dst})
         copy.start()
         mixed_copies.append(copy)
 
@@ -424,19 +437,15 @@
         kc = col_k[h]
         keep, correction = vec[2, h], vec[3, h]
         for s in range(own):
-            state[s, h] = (
+            next_state[s, h] = (
                 keep[s : s + 1] * state[s, h] + kc[:, s : s + 1] * correction[s : s + 1]
             )
         return carry
 
     lax.fori_loop(0, H, update, 0)
     load_mix.wait()
-    for d in range(1, G):
-        remote(
-            mixed_all.at[k], mixed_all.at[source(d)], mixed_sem, d - 1, d - 1, partner
-        ).wait_recv()
-    store_state = pltpu.make_async_copy(state, next_state, store_sem.at[0])
-    store_state.start()
+    for src in nearest:
+        remote(mixed_all.at[k], mixed_all.at[src], mixed_sem, 0, src, partner).wait_recv()
     mixed = jnp.concatenate([mixed_all[j].astype(F32) for j in range(G)], axis=0).astype(BF16)
     attn_out[...] = jnp.dot(
         mixed, wm[:, pl.ds(pl.multiple_of(other * F, F), F)], preferred_element_type=F32
@@ -451,8 +460,8 @@
     middle[...] = mid
     mid_all[k] = mid
     mid_copies = []
-    for d in offsets:
-        copy = remote(middle, mid_all.at[k], mid_sem, d - 1, d - 1, {"kv": peer(d)})
+    for j, dst in enumerate(others):
+        copy = remote(middle, mid_all.at[k], mid_sem, j, k, {"kv": dst})
         copy.start()
         mid_copies.append(copy)
 
@@ -461,14 +470,12 @@
     squares = jnp.zeros((R, 1), F32)
     load_gate.wait()
     load_up.wait()
-    for d, copy in gain_copies:
-        remote(gain_out, gain_all.at[source(d)], gain_sem, d - 1, d - 1, partner).wait_recv()
-    order = [0] + sorted(range(1, G), key=lambda d: min(d, G - d))
+    for src in nearest:
+        remote(gain_out, gain_all.at[src], gain_sem, 0, src, partner).wait_recv()
     gu_copies = []
-    for position, d in enumerate(order):
-        src = source(d) if d else k
-        if d:
-            remote(middle, mid_all.at[src], mid_sem, d - 1, d - 1, partner).wait_recv()
+    for position, src in enumerate([k] + nearest):
+        if position:
+            remote(middle, mid_all.at[src], mid_sem, 0, src, partner).wait_recv()
         x = mid_all[src].astype(F32)
         squares = squares + jnp.sum(x * x, axis=1, keepdims=True)
         x = (x * gain_all[src][0:1]).astype(BF16)
@@ -502,36 +509,27 @@
         pieces.append((jax.nn.silu(gate) * up).astype(BF16))
     load_down.wait()
     down_copies = []
-    for d in offsets + [0]:
-        dst = peer(d) if d else k
+    for j, dst in enumerate(others + [k]):
         cols = pl.ds(pl.multiple_of(dst * F, F), F)
         value = sum(
             jnp.dot(piece, wdown[span, cols], preferred_element_type=F32)
             for piece, span in zip(pieces, spans)
         )
-        if d:
-            down_out[d - 1] = value.astype(BF16)
-            copy = remote(
-                down_out.at[d - 1], down_in.at[d - 1], down_sem, d - 1, d - 1, {"kv": dst}
-            )
+        if j < G - 1:
+            down_out[j] = value.astype(BF16)
+            copy = remote(down_out.at[j], down_in.at[k], down_sem, j, k, {"kv": dst})
             copy.start()
             down_copies.append(copy)
     total = value
-    for d in sorted(range(1, G), key=lambda d: min(d, G - d)):
-        remote(down_out.at[d - 1], down_in.at[d - 1], down_sem, d - 1, d - 1, partner).wait_recv()
-        total = total + down_in[d - 1].astype(F32)
-    out_buf[...] = (middle[...].astype(F32) + total).astype(BF16)
-    store_out = pltpu.make_async_copy(out_buf, layer_out, store_sem.at[1])
-    store_out.start()
+    for src in nearest:
+        remote(down_out.at[0], down_in.at[src], down_sem, 0, src, partner).wait_recv()
+        total = total + down_in[src].astype(F32)
+    layer_out[...] = (middle[...].astype(F32) + total).astype(BF16)
     send_tok.wait_send()
-    for d, copy in gain_copies:
-        copy.wait_send()
-    for copy in proj_copies + mixed_copies + mid_copies + gu_copies + down_copies:
+    for copy in gain_copies + proj_copies + mixed_copies + mid_copies + gu_copies + down_copies:
         copy.wait_send()
     send_attn.wait_send()
     send_sq.wait_send()
-    store_state.wait()
-    store_out.wait()
 
 
 def one_kernel(
@@ -565,11 +563,11 @@
     return pl.pallas_call(
         functools.partial(layer_kernel, G),
         out_shape=(
-            jax.ShapeDtypeStruct(tokens.shape, BF16),
-            jax.ShapeDtypeStruct(delta_state.shape, F32),
+            pltpu.VMEM(tokens.shape, BF16),
+            pltpu.VMEM(delta_state.shape, F32),
         ),
         in_specs=[pl.BlockSpec(memory_space=pltpu.SMEM)] + [inside] * 3 + [anywhere] * 12,
-        out_specs=(anywhere, anywhere),
+        out_specs=(inside, inside),
         scratch_shapes=[
             pltpu.VMEM((2, R, F), BF16),
             vmem(delta_state),
@@ -577,17 +575,17 @@
             vmem(w_key),
             vmem(w_value),
             vmem(w_out_gate),
-            vmem(w_beta),
-            vmem(w_decay),
+            pltpu.VMEM(w_beta.shape[::-1], BF16),
+            pltpu.VMEM(w_decay.shape[::-1], BF16),
             vmem(w_mix),
             vmem(w_gate),
             vmem(w_up),
             vmem(w_down),
             pltpu.VMEM((R, 4 * C), F32),
             pltpu.VMEM((2, G, own, 2 * C), BF16),
-            pltpu.VMEM((2, G - 1, own, 2 * C), BF16),
+            pltpu.VMEM((2, G, own, 2 * C), BF16),
             pltpu.VMEM((G, own, 128), F32),
-            pltpu.VMEM((G - 1, own, 128), F32),
+            pltpu.VMEM((G, own, 128), F32),
             pltpu.VMEM((8, F), F32),
             pltpu.VMEM((G, 8, F), F32),
             pltpu.VMEM((H, HEAD_DIM, own), F32),
@@ -604,20 +602,20 @@
             pltpu.VMEM((R, 128), F32),
             pltpu.VMEM((R, 128), F32),
             pltpu.VMEM((G - 1, R, F), BF16),
-            pltpu.VMEM((G - 1, R, F), BF16),
-            pltpu.VMEM((R, F), BF16),
+            pltpu.VMEM((G, R, F), BF16),
+            pltpu.VMEM((1, 2 * F), F32),
+            pltpu.VMEM((1, 2 * F), F32),
             dma((12,)),
             dma((2, 1)),
-            dma((2, G - 1)),
-            dma((2, 2 * (G - 1))),
-            dma((2, G - 1)),
-            dma((2, G - 1)),
+            dma((2, G)),
+            dma((2, 2 * G)),
+            dma((2, G)),
+            dma((2, G)),
             dma((2, 1)),
-            dma((2, G - 1)),
+            dma((2, G)),
             dma((2, 2)),
             dma((2, 1)),
-            dma((2, G - 1)),
-            dma((2,)),
+            dma((2, G)),
         ],
         compiler_params=pltpu.CompilerParams(
             collective_id=0, has_side_effects=True, vmem_limit_bytes=60 * 2**20
@@ -625,16 +623,16 @@
     )(
         decay_rate,
         head_gain.reshape(1, -1),
-        gain_in.reshape(1, -1),
-        gain_mid.reshape(1, -1),
+        gain_in.reshape(-1, 128),
+        gain_mid.reshape(-1, 128),
         tokens,
         delta_state,
         w_query,
         w_key,
         w_value,
         w_out_gate,
-        w_beta,
-        w_decay,
+        w_beta.T,
+        w_decay.T,
         w_mix,
         w_gate,
         w_up,

time: 40 us -> 29.7 us (0.74)
  local copies, waits for them, and re-layouts: 9.98 us -> 1.93 us
  Pallas kernels: 28.9 us -> 26.9 us
    unnamed x4 -> x2, local copies, waits for them, and re-layouts: 7.45 us -> 1.93 us
    reshape x2 -> x0, local copies, waits for them, and re-layouts: 2.53 us -> none  [the longest x1 1.27 us: one_kernel(): gain_mid.reshape(1, -1)]
    pallas_call x1, Pallas kernels: 28.9 us -> 26.9 us  [one_kernel(): pl.pallas_call(functools.partial(layer_kernel, G), out_shape=(pltpu.VMEM(...]
where the time goes in v2:
time: 29.7 us; the launch traced here: 29.5 us
  Pallas kernels  26.9 us (91%)
  local copies, waits for them, and re-layouts  1.93 us (6%)
  between operations  0.65 us (2%)
    pallas_call x1, Pallas kernels, one_kernel(): pl.pallas_call(functools.partial(layer_kernel, G), out_shape=(pltpu.VMEM(...  26.9 us
    unnamed x2, local copies, waits for them, and re-layouts  1.93 us

profile of v2, /device:TPU:0, one launch (start us, length us, event | category | flops | bytes accessed | tf_op | source)
XLA Modules:
  0.0 29.5 jit_solution(10903919662604642256)
XLA Ops:
  0.6 26.9 %shard_map.167 = (bf16[32,256]{1,0:T(8,128)(2,1)S(1)}, f32[8,4,128,128]{3,2,1,0:T(8,128)S(1)}) custom-call(f32[4]{0:T(128)} %decay_rate.1, f32[1,128]{1,0:T(1,128)} %bitcast.9, bf16[4,128]{1,0:T(4,128)(2,1)} %bitcast.7, bf16[4,128]{1,0:T(4,128)(2,1)} %bitcast.8, bf16[32,256]{1,0:T(8,128)(2,1)} %tokens.1, f32[8,4,128,128]{3,2,1,0:T(8,128)} %delta_state.1, ...), custom_call_target="tpu_custom_call" | custom-call | tf_op jit(solution)/shard_map/pallas_call | solution.py:563
  27.6 0.6 %copy.20 = bf16[32,256]{1,0:T(8,128)(2,1)} copy(bf16[32,256]{1,0:T(8,128)(2,1)S(1)} %get-tuple-element.2) | data formatting | bytes 32768
  28.2 1.3 %copy.21 = f32[8,4,128,128]{3,2,1,0:T(8,128)} copy(f32[8,4,128,128]{3,2,1,0:T(8,128)S(1)} %get-tuple-element.3) | data formatting | bytes 4194304

commit v3 on v2

--- a/solution.py
+++ b/solution.py
@@ -161,10 +161,10 @@
 
 def layer_kernel(
     G,
-    decay_rate,
-    head_gain,
-    gain_in,
-    gain_mid,
+    decay_hbm,
+    head_hbm,
+    gain_in_hbm,
+    gain_mid_hbm,
     tokens,
     delta_state,
     w_query,
@@ -202,8 +202,7 @@
     col_q,
     vec,
     mixed_all,
-    attn_out,
-    attn_in,
+    wm_two,
     mid_all,
     middle,
     acc,
@@ -215,6 +214,10 @@
     down_in,
     gain_row_in,
     gain_row_mid,
+    decay_rate,
+    head_gain,
+    gain_in,
+    gain_mid,
     load_sem,
     tok_sem,
     gain_sem,
@@ -268,10 +271,22 @@
         )
 
     load_tok = load(tokens, tok.at[t])
+    load_small = [
+        load(a, b)
+        for a, b in (
+            (gain_in_hbm, gain_in),
+            (gain_mid_hbm, gain_mid),
+            (head_hbm, head_gain),
+            (decay_hbm, decay_rate),
+        )
+    ]
     barrier = pltpu.get_barrier_semaphore()
     pl.semaphore_signal(barrier, inc=1, device_id=partner, device_id_type=MESH)
     for dst in others:
-        pl.semaphore_signal(barrier, inc=1, device_id={"kv": dst}, device_id_type=MESH)
+        for core in (t, other):
+            pl.semaphore_signal(
+                barrier, inc=1, device_id={"kv": dst, "tp": core}, device_id_type=MESH
+            )
     load_proj = [
         load(a, b)
         for a, b in (
@@ -284,13 +299,15 @@
         )
     ]
 
+    for copy in load_small:
+        copy.wait()
     gain_row_in[...] = as_row(gain_in[...])
     gain_row_mid[...] = as_row(gain_mid[...])
     gain_mid_own = gain_row_mid[:, pl.ds(pl.multiple_of(t * F, F), F)]
     gain_out[...] = jnp.broadcast_to(gain_mid_own, gain_out.shape)
     gain_all[k] = jnp.broadcast_to(gain_mid_own, gain_out.shape)
     load_tok.wait()
-    pl.semaphore_wait(barrier, G)
+    pl.semaphore_wait(barrier, 2 * G - 1)
 
     send_tok = remote(tok.at[t], tok.at[t], tok_sem, 0, 0, partner)
     send_tok.start()
@@ -317,8 +334,8 @@
             part[:, i * C : (i + 1) * C] = jnp.dot(
                 x_own, weights[i][rows_of(t), :], preferred_element_type=F32
             )
+    load_mix = load(w_mix, wm)
     load_state = load(delta_state, state)
-    load_mix = load(w_mix, wm)
     load_gate = load(w_gate, wgate)
     load_up = load(w_up, wup)
     load_down = load(w_down, wdown)
@@ -359,6 +376,11 @@
                 copy = remote(extra_out.at[dst], extra_in.at[k], extra_sem, j, k, {"kv": dst})
                 copy.start()
                 proj_copies.append(copy)
+    load_mix.wait()
+    send_mix = remote(
+        wm.at[:, pl.ds(pl.multiple_of(other * F, F), F)], wm_two, attn_sem, 0, 0, partner
+    )
+    send_mix.start()
     own_rows = pl.ds(pl.multiple_of(k * own, own), own)
     sum_extra = extra_out[k]
     for src in nearest:
@@ -412,7 +434,7 @@
         vec[4, h] = jnp.concatenate(asked, axis=0)
         return carry
 
-    lax.fori_loop(0, H, recall, 0)
+    lax.fori_loop(0, H, recall, 0, unroll=True)
     value_gate = chunk_sum(1)
     gain_row = head_gain[...]
     for h in range(H):
@@ -426,12 +448,25 @@
         readout = readout * lax.rsqrt(
             jnp.mean(readout * readout, axis=-1, keepdims=True) + norm_epsilon
         )
-        mixed_all[k, :, cols] = (readout * gain_row * gate).astype(BF16)
+        mixed_all[t, k, :, cols] = (readout * gain_row * gate).astype(BF16)
     mixed_copies = []
     for j, dst in enumerate(others):
-        copy = remote(mixed_all.at[k], mixed_all.at[k], mixed_sem, j, k, {"kv": dst})
-        copy.start()
-        mixed_copies.append(copy)
+        for c, core in enumerate((t, other)):
+            copy = remote(
+                mixed_all.at[t, k],
+                mixed_all.at[t, k],
+                mixed_sem,
+                2 * j + c,
+                t * G + k,
+                {"kv": dst, "tp": core},
+            )
+            copy.start()
+            mixed_copies.append(copy)
+    copy = remote(
+        mixed_all.at[t, k], mixed_all.at[t, k], mixed_sem, 2 * G - 2, t * G + k, partner
+    )
+    copy.start()
+    mixed_copies.append(copy)
 
     def update(h, carry):
         kc = col_k[h]
@@ -442,21 +477,21 @@
             )
         return carry
 
-    lax.fori_loop(0, H, update, 0)
-    load_mix.wait()
-    for src in nearest:
-        remote(mixed_all.at[k], mixed_all.at[src], mixed_sem, 0, src, partner).wait_recv()
-    mixed = jnp.concatenate([mixed_all[j].astype(F32) for j in range(G)], axis=0).astype(BF16)
-    attn_out[...] = jnp.dot(
-        mixed, wm[:, pl.ds(pl.multiple_of(other * F, F), F)], preferred_element_type=F32
-    ).astype(BF16)
-    send_attn = remote(attn_out, attn_in, attn_sem, 0, 0, partner)
-    send_attn.start()
-    attn = jnp.dot(
-        mixed, wm[:, pl.ds(pl.multiple_of(t * F, F), F)], preferred_element_type=F32
-    ).astype(BF16)
-    send_attn.wait_recv()
-    mid = (tok[t].astype(F32) + (attn.astype(F32) + attn_in[...].astype(F32))).astype(BF16)
+    lax.fori_loop(0, H, update, 0, unroll=True)
+    send_mix.wait_recv()
+
+    def half_product(core, sources, weight):
+        for src in sources:
+            remote(
+                mixed_all.at[t, k], mixed_all.at[core, src], mixed_sem, 0, core * G + src, partner
+            ).wait_recv()
+        mixed = jnp.concatenate([mixed_all[core, j].astype(F32) for j in range(G)], axis=0)
+        product = jnp.dot(mixed.astype(BF16), weight, preferred_element_type=F32)
+        return product.astype(BF16).astype(F32)
+
+    attn = half_product(t, nearest, wm[:, pl.ds(pl.multiple_of(t * F, F), F)])
+    attn = attn + half_product(other, [k] + nearest, wm_two[...])
+    mid = (tok[t].astype(F32) + attn).astype(BF16)
     middle[...] = mid
     mid_all[k] = mid
     mid_copies = []
@@ -528,7 +563,7 @@
     send_tok.wait_send()
     for copy in gain_copies + proj_copies + mixed_copies + mid_copies + gu_copies + down_copies:
         copy.wait_send()
-    send_attn.wait_send()
+    send_mix.wait_send()
     send_sq.wait_send()
 
 
@@ -566,7 +601,7 @@
             pltpu.VMEM(tokens.shape, BF16),
             pltpu.VMEM(delta_state.shape, F32),
         ),
-        in_specs=[pl.BlockSpec(memory_space=pltpu.SMEM)] + [inside] * 3 + [anywhere] * 12,
+        in_specs=[anywhere] * 16,
         out_specs=(inside, inside),
         scratch_shapes=[
             pltpu.VMEM((2, R, F), BF16),
@@ -591,9 +626,8 @@
             pltpu.VMEM((H, HEAD_DIM, own), F32),
             pltpu.VMEM((H, HEAD_DIM, own), F32),
             pltpu.VMEM((5, H, own, HEAD_DIM), F32),
-            pltpu.VMEM((G, own, C), BF16),
-            pltpu.VMEM((R, F), BF16),
-            pltpu.VMEM((R, F), BF16),
+            pltpu.VMEM((2, G, own, C), BF16),
+            pltpu.VMEM((C, F), BF16),
             pltpu.VMEM((G, R, F), BF16),
             pltpu.VMEM((R, F), BF16),
             pltpu.VMEM((2, R, HID), F32),
@@ -605,12 +639,16 @@
             pltpu.VMEM((G, R, F), BF16),
             pltpu.VMEM((1, 2 * F), F32),
             pltpu.VMEM((1, 2 * F), F32),
-            dma((12,)),
+            pltpu.SMEM((H,), F32),
+            pltpu.VMEM((1, HEAD_DIM), F32),
+            pltpu.VMEM((2 * F // 128, 128), BF16),
+            pltpu.VMEM((2 * F // 128, 128), BF16),
+            dma((16,)),
             dma((2, 1)),
             dma((2, G)),
             dma((2, 2 * G)),
             dma((2, G)),
-            dma((2, G)),
+            dma((2, 2 * G)),
             dma((2, 1)),
             dma((2, G)),
             dma((2, 2)),

time: 29.7 us -> 28 us (0.943)
  Pallas kernels: 26.9 us -> 25.1 us
    pallas_call x1, Pallas kernels: 26.9 us -> 25.1 us  [one_kernel(): pl.pallas_call(functools.partial(layer_kernel, G), out_shape=(pltpu.VMEM(...]
where the time goes in v3:
time: 28 us; the launch traced here: 27.7 us
  Pallas kernels  25.1 us (90%)
  local copies, waits for them, and re-layouts  1.93 us (7%)
  between operations  0.65 us (2%)
    pallas_call x1, Pallas kernels, one_kernel(): pl.pallas_call(functools.partial(layer_kernel, G), out_shape=(pltpu.VMEM(...  25.1 us
    unnamed x2, local copies, waits for them, and re-layouts  1.93 us

profile of v3, /device:TPU:0, one launch (start us, length us, event | category | flops | bytes accessed | tf_op | source)
XLA Modules:
  0.0 27.7 jit_solution(13876944453366319652)
XLA Ops:
  0.6 25.1 %shard_map.167 = (bf16[32,256]{1,0:T(8,128)(2,1)S(1)}, f32[8,4,128,128]{3,2,1,0:T(8,128)S(1)}) custom-call(f32[4]{0:T(128)} %decay_hbm.1, f32[1,128]{1,0:T(1,128)} %bitcast.9, bf16[4,128]{1,0:T(4,128)(2,1)} %bitcast.7, bf16[4,128]{1,0:T(4,128)(2,1)} %bitcast.8, bf16[32,256]{1,0:T(8,128)(2,1)} %tokens.1, f32[8,4,128,128]{3,2,1,0:T(8,128)} %delta_state.1, ...), custom_call_target="tpu_custom_call" | custom-call | tf_op jit(solution)/shard_map/pallas_call | solution.py:598
  25.8 0.6 %copy.20 = bf16[32,256]{1,0:T(8,128)(2,1)} copy(bf16[32,256]{1,0:T(8,128)(2,1)S(1)} %get-tuple-element.2) | data formatting | bytes 32768
  26.4 1.3 %copy.21 = f32[8,4,128,128]{3,2,1,0:T(8,128)} copy(f32[8,4,128,128]{3,2,1,0:T(8,128)S(1)} %get-tuple-element.3) | data formatting | bytes 4194304
